TPU v7x, 32 devices: a whole 2x2x4 slice. The times are simulated.
32 devices in a mesh: fs: 8 (over z, x), tp: 4 (over y, core).
Axes of the slice: x: 2, y: 2, z: 4, core: 2. Of those that a mesh axis runs over, the one named last changes fastest.
Arguments:
- tokens: bfloat16 [3072, 4096], P('fs', 'tp'), may hold values from -600 to 600
- gate_master: float32 [8, 4096, 512], P(None, 'fs', 'tp'), may hold values from -0.09375 to 0.09375
- up_master: float32 [8, 4096, 512], P(None, 'fs', 'tp'), may hold values from -0.09375 to 0.09375
- down_master: float32 [8, 4096, 512], P(None, 'fs', 'tp'), may hold values from -0.25 to 0.25
- norm_gain: float32 [4096], P('fs'), may hold values from 0.1 to 1.9
- routes: int32 [3072, 2], P('fs'), may hold values from 0 to 7, all different within a row; in each aligned block of 384 rows (0 to 383, 384 to 767, ...) at most 192 rows name the same one
- route_weight: float32 [3072, 2], P('fs'), may hold values from 0.1 to 1
Outputs:
- gate_out: bfloat16 [8, 4096, 512], P('fs', None, 'tp')
- up_out: bfloat16 [8, 4096, 512], P('fs', None, 'tp')
- down_out: bfloat16 [8, 4096, 512], P('fs', None, 'tp')
- mixed: bfloat16 [3072, 4096], P('fs', 'tp')
Inputs may be any that keep to these rules, and one draw needn't show every extreme that they name: `routes`: within the rows of one index of fs no expert is named by more than 192 pairs, a bound that some block reaches; the 2 experts of a row differ.
All inputs are finite; a program needn't handle non-finite values.
Results may differ from a plain program's by a relative error of at most 0.0087.
Values may be sent and summed in bfloat16 or wider, within the bound.
No kernel may reach another device: no remote copies, remote signals or barrier semaphores. Data moves between devices by JAX's collectives and lax.ppermute only.
A program may use at most 128 MiB of HBM per device.

v0:
```python
import jax
import jax.numpy as jnp
from jax import lax
from jax.sharding import PartitionSpec as P

norm_eps = 1e-06


def slot_table(expert_ids, n_experts, capacity, top_count):
    assigned = expert_ids.shape[0]
    onehot = (expert_ids[:, None] == jnp.arange(n_experts, dtype=jnp.int32)[None, :]).astype(
        jnp.int32
    )
    before = jnp.cumsum(onehot, axis=0) - onehot
    slots = jnp.sum(before * onehot, axis=1)
    position = expert_ids * capacity + slots
    owners = jnp.arange(assigned, dtype=jnp.int32) // top_count
    matches = position[None, :] == jnp.arange(n_experts * capacity, dtype=jnp.int32)[:, None]
    slot_token = jnp.max(jnp.where(matches, owners[None, :], -1), axis=1)
    return (position, slot_token)


def place_rows(normed, slot_token):
    padded = jnp.concatenate([normed, jnp.zeros((1, normed.shape[1]), normed.dtype)], axis=0)
    chosen = jnp.where(slot_token < 0, normed.shape[0], slot_token)
    return padded[chosen]


def body(tokens, gate_master, up_master, down_master, norm_gain, routes, route_weight):
    n_experts = gate_master.shape[0]
    tok_rows = routes.shape[0]
    top_count = routes.shape[1]
    capacity = 2 * tok_rows * top_count // n_experts
    folded = norm_gain[None, :, None]
    gate_cast = (gate_master * folded).astype(jnp.bfloat16)
    up_cast = (up_master * folded).astype(jnp.bfloat16)
    down_cast = down_master.astype(jnp.bfloat16)
    gate_out, up_out, down_out = (
        lax.all_to_all(gate_cast, "fs", split_axis=0, concat_axis=1, tiled=True),
        lax.all_to_all(up_cast, "fs", split_axis=0, concat_axis=1, tiled=True),
        lax.all_to_all(down_cast, "fs", split_axis=0, concat_axis=1, tiled=True),
    )
    flat_routes = routes.reshape(-1)
    position, slot_token = slot_table(flat_routes, n_experts, capacity, top_count)
    mix_weights = route_weight / jnp.sum(route_weight, axis=1, keepdims=True)
    gate_mat = gate_out[0]
    up_mat = up_out[0]
    token_float = tokens.astype(jnp.float32)
    full_width = token_float.shape[1] * lax.axis_size("tp")
    sumsquares = lax.psum(jnp.sum(token_float * token_float, axis=1), "tp")
    inverse = lax.rsqrt(sumsquares / full_width + norm_eps)[:, None]
    normed = (token_float * inverse).astype(jnp.bfloat16)
    outgoing = place_rows(normed, slot_token).reshape(n_experts, capacity, normed.shape[1])
    arrived = lax.all_to_all(outgoing, "fs", split_axis=0, concat_axis=0, tiled=True).reshape(
        -1, normed.shape[1]
    )
    segment = lax.all_gather(arrived, "tp", axis=1, tiled=True)
    gate_val = jnp.dot(segment, gate_mat, preferred_element_type=jnp.float32)
    up_val = jnp.dot(segment, up_mat, preferred_element_type=jnp.float32)
    hidden = (jax.nn.silu(gate_val) * up_val).astype(jnp.bfloat16)
    hidden_whole = lax.all_gather(hidden, "tp", axis=1, tiled=True)
    down_quarter = lax.all_to_all(down_out[0], "tp", split_axis=0, concat_axis=1, tiled=True)
    result = lax.dot_general(
        hidden_whole, down_quarter, (((1,), (1,)), ((), ())), preferred_element_type=jnp.float32
    )
    summed = result.astype(jnp.bfloat16)
    returned = lax.all_to_all(
        summed.reshape(-1, capacity, summed.shape[1]), "fs", split_axis=0, concat_axis=0, tiled=True
    )
    flat_back = returned.reshape(-1, summed.shape[1])
    picked = flat_back[position].astype(jnp.float32).reshape(tok_rows, top_count, summed.shape[1])
    mixed = jnp.sum(mix_weights[:, :, None] * picked, axis=1).astype(jnp.bfloat16)
    return (gate_out, up_out, down_out, mixed)


def solution(mesh):
    placed = (
        P("fs", "tp"),
        P(None, "fs", "tp"),
        P(None, "fs", "tp"),
        P(None, "fs", "tp"),
        P("fs"),
        P("fs", None),
        P("fs", None),
    )
    return jax.shard_map(
        body,
        mesh=mesh,
        in_specs=placed,
        out_specs=(P("fs", None, "tp"), P("fs", None, "tp"), P("fs", None, "tp"), P("fs", "tp")),
        check_vma=False,
    )
```

profile of v0, /device:TPU:0, one launch (start us, length us, event | category | flops | bytes accessed | tf_op | source)
XLA Modules:
  0.0 341.4 jit_solution(13418795608480970905)
XLA Ops:
  8.3 1.7 reduce-window.6
  11.4 1.4 fusion.1
  12.7 8.4 %psum.7 = f32[384]{0:T(512)S(1)} all-reduce(f32[384]{0:T(512)S(1)} %fusion.1), channel_id=1, replica_groups=mesh['fs'=8,'tp'=4] {'tp'}, use_global_device_ids=true, to_apply=%region_2.3 | all-reduce | flops 384 | bytes 3072 | tf_op jit(solution)/shard_map/psum | solution.py:50
  21.1 1.3 fusion.2
  22.5 5.8 %gather_fusion = bf16[1536,1024]{1,0:T(8,128)(2,1)} fusion(bf16[385,1024]{1,0:T(8,128)(2,1)S(1)} %concatenate.3, s32[2048]{0:T(1024)S(1)} %pad_clamp_fusion), kind=kCustom, calls=%fused_computation | custom fusion | bytes 6297600 | tf_op jit(solution)/shard_map/gather | solution.py:26
  28.4 75.4 %all_to_all.65 = bf16[8,192,1024]{2,1,0:T(8,128)(2,1)} all-to-all(bf16[8,192,1024]{2,1,0:T(8,128)(2,1)} %bitcast.30), channel_id=1, replica_groups=mesh['fs'=8,'tp'=4] {'fs'}, dimensions={0} | all-to-all | bytes 6291456 | tf_op jit(solution)/shard_map/all_to_all | solution.py:54
  103.8 1.6 copy-done.6
  105.4 3.0 multiply_convert_fusion
  108.3 28.8 %all_to_all.66 = bf16[8,512,128]{2,1,0:T(8,128)(2,1)S(1)} all-to-all(bf16[8,512,128]{2,1,0:T(8,128)(2,1)S(1)} %get-tuple-element.5), channel_id=1, replica_groups=mesh['fs'=8,'tp'=4] {'fs'}, dimensions={0} | all-to-all | bytes 2097152 | tf_op jit(solution)/shard_map/all_to_all | solution.py:39
  137.1 3.6 %all-to-all-start.1 = ((bf16[8,512,128]{2,1,0:T(8,128)(2,1)}), bf16[8,512,128]{2,1,0:T(8,128)(2,1)S(1)}, u32[]{:S(2)}, u32[]{:S(2)}) async-start(bf16[8,512,128]{2,1,0:T(8,128)(2,1)} %get-tuple-element.4), calls=%async_computation.1 | async-start | bytes 2097152 | tf_op jit(solution)/shard_map/all_to_all | solution.py:40
  140.7 2.7 convert_element_type.40
  143.4 41.7 %all-gather.3.cloned.1.call-done = bf16[1536,4096]{1,0:T(8,128)(2,1)} async-done(((bf16[1536,1024]{1,0:T(8,128)(2,1)}), bf16[1536,4096]{1,0:T(8,128)(2,1)}) %all-gather.3.cloned.1.call-update) | async-done | bytes 12582928 | tf_op jit(solution)/shard_map/all_gather | solution.py:57
  185.1 6.4 %fusion.11 = f32[1536,128]{1,0:T(8,128)S(1)} fusion(bf16[1536,4096]{1,0:T(8,128)(2,1)} %all-gather.3.cloned.1.call-done, bf16[4096,128]{1,0:T(8,128)(2,1)S(1)} %bitcast.33), kind=kOutput, calls=%fused_computation.38 | convolution fusion | flops 1610612736 | bytes 14417920 | tf_op jit(solution)/shard_map/dot_general | solution.py:58
  191.5 5.5 %all-to-all-start.2 = ((bf16[8,512,128]{2,1,0:T(8,128)(2,1)}), bf16[8,512,128]{2,1,0:T(8,128)(2,1)S(1)}, u32[]{:S(2)}, u32[]{:S(2)}) async-start(bf16[8,512,128]{2,1,0:T(8,128)(2,1)} %convert_element_type.40), calls=%async_computation.2 | async-start | bytes 2097152 | tf_op jit(solution)/shard_map/all_to_all | solution.py:41
  197.1 7.4 %fusion = bf16[1536,128]{1,0:T(8,128)(2,1)} fusion(bf16[1536,4096]{1,0:T(8,128)(2,1)} %all-gather.3.cloned.1.call-done, bf16[4096,128]{1,0:T(8,128)(2,1)S(1)} %bitcast.35, f32[1536,128]{1,0:T(8,128)S(1)} %fusion.11), kind=kOutput, calls=%fused_computation.7 | convolution fusion | flops 1611792384 | bytes 14811136 | tf_op jit(solution)/shard_map/dot_general | solution.py:59
  204.5 18.7 %all-to-all-done.2 = bf16[8,512,128]{2,1,0:T(8,128)(2,1)S(1)} async-done(((bf16[8,512,128]{2,1,0:T(8,128)(2,1)}), bf16[8,512,128]{2,1,0:T(8,128)(2,1)S(1)}, u32[]{:S(2)}, u32[]{:S(2)}) %all-to-all-start.2) | async-done | bytes 1048608 | tf_op jit(solution)/shard_map/all_to_all | solution.py:41
  223.3 16.8 %all_to_all.67 = bf16[4,1024,128]{2,1,0:T(8,128)(2,1)S(1)} all-to-all(bf16[4,1024,128]{2,1,0:T(8,128)(2,1)S(1)} %bitcast.31), channel_id=1, replica_groups=mesh['fs'=8,'tp'=4] {'tp'}, dimensions={0} | all-to-all | bytes 2097152 | tf_op jit(solution)/shard_map/all_to_all | solution.py:62
  240.7 4.9 %convolution_convert_fusion = bf16[1536,1024]{1,0:T(8,128)(2,1)} fusion(bf16[1536,512]{1,0:T(8,128)(2,1)} %all-gather.5.cloned.1.call-done, bf16[1024,512]{0,1:T(8,128)(2,1)S(1)} %bitcast.39), kind=kOutput, calls=%fused_computation.4 | convolution fusion | flops 1612185600 | bytes 5767168 | tf_op jit(solution)/shard_map/dot_general | solution.py:63
  245.5 4.0 %all-to-all-start.5 = ((bf16[8,192,1024]{2,1,0:T(8,128)(2,1)}), bf16[8,192,1024]{2,1,0:T(8,128)(2,1)S(1)}, u32[]{:S(2)}, u32[]{:S(2)}) async-start(bf16[8,192,1024]{2,1,0:T(8,128)(2,1)} %bitcast.38), calls=%async_computation.5 | async-start | bytes 6291456 | tf_op jit(solution)/shard_map/all_to_all | solution.py:67
  250.1 69.8 %all-to-all-done.5 = bf16[8,192,1024]{2,1,0:T(8,128)(2,1)S(1)} async-done(((bf16[8,192,1024]{2,1,0:T(8,128)(2,1)}), bf16[8,192,1024]{2,1,0:T(8,128)(2,1)S(1)}, u32[]{:S(2)}, u32[]{:S(2)}) %all-to-all-start.5) | async-done | bytes 3145760 | tf_op jit(solution)/shard_map/all_to_all | solution.py:67
  319.9 3.6 %gather_fusion.1 = bf16[768,1024]{1,0:T(8,128)(2,1)} fusion(bf16[1536,1024]{1,0:T(8,128)(2,1)S(1)} %bitcast.28, s32[1024]{0:T(1024)S(1)} %pad_clamp_fusion.1), kind=kCustom, calls=%fused_computation.1 | custom fusion | bytes 3148800 | tf_op jit(solution)/shard_map/gather | solution.py:71
  323.4 3.4 reshape.138
  326.9 4.8 %multiply_reduce_fusion = bf16[384,1024]{1,0:T(8,128)(2,1)} fusion(f32[384,2,1024]{2,1,0:T(2,128)S(1)} %reshape.138, f32[384,2]{1,0:T(8,128)S(1)} %copy.27), kind=kLoop, calls=%fused_computation.5 | loop fusion | flops 1179648 | bytes 3935232 | tf_op jit(solution)/shard_map/reduce_sum | solution.py:72
  331.7 1.0 copy.37
  (51 shorter events, 5.6 us)
Async XLA Ops:
  7.2 177.9 %all-gather.3.cloned.1.call-start = ((), (), s32[]{:S(2)}) async-start(), calls=%async_computation.6 | async-start | bytes 15728640 | tf_op jit(solution)/shard_map/all_gather | solution.py:57
  103.8 1.6 copy-start.6
  103.8 1.6 copy-start.9
  137.1 54.4 %copy-start.2 = (bf16[8,512,128]{2,1,0:T(8,128)(2,1)}, bf16[8,512,128]{2,1,0:T(8,128)(2,1)S(1)}, u32[]{:S(2)}) copy-start(bf16[8,512,128]{2,1,0:T(8,128)(2,1)S(1)} %all_to_all.66) | copy-start | bytes 3145732
  137.1 54.4 %all-to-all-start.1 = ((bf16[8,512,128]{2,1,0:T(8,128)(2,1)}), bf16[8,512,128]{2,1,0:T(8,128)(2,1)S(1)}, u32[]{:S(2)}, u32[]{:S(2)}) async-start(bf16[8,512,128]{2,1,0:T(8,128)(2,1)} %get-tuple-element.4), calls=%async_computation.1 | async-start | bytes 2097152 | tf_op jit(solution)/shard_map/all_to_all | solution.py:40
  191.5 13.0 %copy-start.4 = (bf16[8,512,128]{2,1,0:T(8,128)(2,1)}, bf16[8,512,128]{2,1,0:T(8,128)(2,1)S(1)}, u32[]{:S(2)}) copy-start(bf16[8,512,128]{2,1,0:T(8,128)(2,1)S(1)} %all-to-all-done.1) | copy-start | bytes 3145732
  191.5 31.7 %all-to-all-start.2 = ((bf16[8,512,128]{2,1,0:T(8,128)(2,1)}), bf16[8,512,128]{2,1,0:T(8,128)(2,1)S(1)}, u32[]{:S(2)}, u32[]{:S(2)}) async-start(bf16[8,512,128]{2,1,0:T(8,128)(2,1)} %convert_element_type.40), calls=%async_computation.2 | async-start | bytes 2097152 | tf_op jit(solution)/shard_map/all_to_all | solution.py:41
  197.1 43.6 %all-gather.5.cloned.1.call-start = ((), (), s32[]{:S(2)}) async-start(), calls=%async_computation.7 | async-start | bytes 1966080 | tf_op jit(solution)/shard_map/all_gather | solution.py:61
  223.3 22.3 %copy-start = (bf16[8,512,128]{2,1,0:T(8,128)(2,1)}, bf16[8,512,128]{2,1,0:T(8,128)(2,1)S(1)}, u32[]{:S(2)}) copy-start(bf16[8,512,128]{2,1,0:T(8,128)(2,1)S(1)} %all-to-all-done.2) | copy-start | bytes 3145732
  245.5 4.0 %copy-start.8 = (s32[384,2]{0,1:T(2,128)S(1)}, s32[384,2]{0,1:T(2,128)}, u32[]{:S(2)}) copy-start(s32[384,2]{0,1:T(2,128)} %param.12) | copy-start | bytes 9220
  245.5 4.3 %copy-start.7 = (f32[384,2]{0,1:T(2,128)S(1)}, f32[384,2]{0,1:T(2,128)}, u32[]{:S(2)}) copy-start(f32[384,2]{0,1:T(2,128)} %param.13) | copy-start | bytes 9220
  245.5 74.3 %all-to-all-start.5 = ((bf16[8,192,1024]{2,1,0:T(8,128)(2,1)}), bf16[8,192,1024]{2,1,0:T(8,128)(2,1)S(1)}, u32[]{:S(2)}, u32[]{:S(2)}) async-start(bf16[8,192,1024]{2,1,0:T(8,128)(2,1)} %bitcast.38), calls=%async_computation.5 | async-start | bytes 6291456 | tf_op jit(solution)/shard_map/all_to_all | solution.py:67
  326.8 4.8 %copy-start.3 = (bf16[8,512,128]{2,1,0:T(8,128)(2,1)S(1)}, bf16[8,512,128]{2,1,0:T(8,128)(2,1)}, u32[]{:S(2)}) copy-start(bf16[8,512,128]{2,1,0:T(8,128)(2,1)} %copy-done.2) | copy-start | bytes 3145732
  326.9 5.8 %copy-start.5 = (bf16[8,512,128]{2,1,0:T(8,128)(2,1)S(1)}, bf16[8,512,128]{2,1,0:T(8,128)(2,1)}, u32[]{:S(2)}) copy-start(bf16[8,512,128]{2,1,0:T(8,128)(2,1)} %copy-done.4) | copy-start | bytes 3145732
  326.9 6.8 %copy-start.1 = (bf16[8,512,128]{2,1,0:T(8,128)(2,1)S(1)}, bf16[8,512,128]{2,1,0:T(8,128)(2,1)}, u32[]{:S(2)}) copy-start(bf16[8,512,128]{2,1,0:T(8,128)(2,1)} %copy-done) | copy-start | bytes 3145732
Sparse Core Ops, SparseCore 0:
  103.9 81.1 all-gather.2
  204.6 20.2 all-gather.4
where the time goes:
time: 342 us; the launch traced here: 341 us
  waiting for transfers between devices  130 us (38%)
  blocking collectives  129 us (38%)
  local copies, waits for them, and re-layouts  19.7 us (6%)
  matrix products  18.6 us (5%)
  other arithmetic  16 us (5%)
  between operations  14.3 us (4%)
  starting transfers between devices  13.1 us (4%)
    all_to_all x1, blocking collectives, body(): lax.all_to_all(outgoing, 'fs', split_axis=0, concat_axis=0, tiled=True)  75.4 us
    all_to_all x1, waiting for transfers between devices, body(): lax.all_to_all(summed.reshape(-1, capacity, summed.shape[1]), 'fs', split...  69.8 us
    all_gather x1, waiting for transfers between devices, body(): segment = lax.all_gather(arrived, 'tp', axis=1, tiled=True)  41.7 us
    all_to_all x1, blocking collectives, body(): lax.all_to_all(gate_cast, 'fs', split_axis=0, concat_axis=1, tiled=True)  28.8 us
    all_to_all x1, waiting for transfers between devices, body(): lax.all_to_all(down_cast, 'fs', split_axis=0, concat_axis=1, tiled=True)  18.7 us
    all_to_all x1, blocking collectives, body(): lax.all_to_all(down_out[0], 'tp', split_axis=0, concat_axis=1, tiled=True)  16.8 us
    psum x1, blocking collectives, body(): sumsquares = lax.psum(jnp.sum(token_float * token_float, axis=1), 'tp')  8.39 us
    dot_general x1, matrix products, body(): up_val = jnp.dot(segment, up_mat, preferred_element_type=jnp.float32)  7.37 us
  transfers between devices with their start and end apart: 5, of which 3 were waited for; matrix products, arithmetic and copies ran while one was open for 6% of the time, Pallas kernels for 0%

commit v1 on v0

v1 whole, which is shorter than its diff:
```python
import jax
import jax.numpy as jnp
from jax import lax
from jax.experimental import pallas as pl
from jax.experimental.pallas import tpu as pltpu
from jax.sharding import PartitionSpec as P

norm_eps = 1e-06
f32 = jnp.float32
bf16 = jnp.bfloat16


def bits_of(n):
    return n.bit_length() - 1


def swap(x, axis, j):
    n = lax.axis_size(axis)
    return lax.ppermute(x, axis, [(s, s ^ j) for s in range(n)])


def reversed_bits(p, n_bits):
    return sum(((p >> k) & 1) << (n_bits - 1 - k) for k in range(n_bits))


def in_kernel(body, out, *args, flops=0):
    nbytes = sum(a.size * a.dtype.itemsize for a in args)
    return pl.pallas_call(
        body,
        out_shape=out,
        in_specs=[pl.BlockSpec(memory_space=pltpu.VMEM)] * len(args),
        out_specs=pl.BlockSpec(memory_space=pltpu.VMEM),
        cost_estimate=pl.CostEstimate(flops=flops, bytes_accessed=nbytes, transcendentals=0),
    )(*args)


def tile_of(rows, most=192):
    t = most
    while rows % t:
        t //= 2
    return t


def up_kernel(r_ref, x_ref, g_ref, u_ref, o_ref):
    rows = x_ref.shape[0]
    n_experts, _, ff = g_ref.shape
    t = tile_of(rows)

    def tile(i, _):
        at = pl.ds(pl.multiple_of(i * t, t), t)
        x = x_ref[at, :]
        first, second = r_ref[at, 0:1], r_ref[at, 1:2]

        def step(e, sums):
            w = jnp.concatenate([g_ref[e], u_ref[e]], axis=1)
            p = jnp.dot(x, w, preferred_element_type=f32)
            return jnp.where(first == e, p, sums[0]), jnp.where(second == e, p, sums[1])

        zero = jnp.zeros((t, 2 * ff), f32)
        a, b = lax.fori_loop(0, n_experts, step, (zero, zero), unroll=n_experts <= 8)
        o_ref[at, : 2 * ff] = a.astype(bf16)
        o_ref[at, 2 * ff :] = b.astype(bf16)
        return 0

    lax.fori_loop(0, rows // t, tile, 0)


def down_kernel(r_ref, h_ref, d_ref, o_ref):
    rows = h_ref.shape[0]
    n_experts, ff, width = d_ref.shape
    t = tile_of(rows)
    zero = jnp.zeros((t, ff), bf16)

    def tile(i, _):
        at = pl.ds(pl.multiple_of(i * t, t), t)
        h = h_ref[at, :]
        first, second = r_ref[at, 0:1], r_ref[at, 1:2]

        def piece(e):
            return jnp.where(first == e, h[:, :ff], jnp.where(second == e, h[:, ff:], zero))

        def step(e, acc):
            pair = jnp.concatenate([piece(2 * e), piece(2 * e + 1)], axis=1)
            w = jnp.concatenate([d_ref[2 * e], d_ref[2 * e + 1]], axis=0)
            return acc + jnp.dot(pair, w, preferred_element_type=f32)

        acc = lax.fori_loop(
            0, n_experts // 2, step, jnp.zeros((t, width), f32), unroll=n_experts <= 8
        )
        o_ref[at, :] = acc.astype(o_ref.dtype)
        return 0

    lax.fori_loop(0, rows // t, tile, 0)


def body(tokens, gate_master, up_master, down_master, norm_gain, routes, route_weight):
    n_fs, n_tp = lax.axis_size("fs"), lax.axis_size("tp")
    i, t = lax.axis_index("fs"), lax.axis_index("tp")
    n_bits = bits_of(n_fs)
    lo = n_fs // n_tp
    n_experts, w, ff = gate_master.shape
    rows, top = routes.shape
    group = rows // n_tp
    place = [reversed_bits(p, n_bits) for p in range(n_fs)]

    folded = norm_gain[None, :, None]
    gate_cast = (gate_master * folded).astype(bf16)
    up_cast = (up_master * folded).astype(bf16)
    down_cast = down_master.astype(bf16)
    down_turned = jnp.swapaxes(down_cast, 1, 2)

    sliced = tokens.reshape(n_tp, group, lo, w).transpose(0, 2, 1, 3)
    mine = [lax.dynamic_index_in_dim(sliced, t ^ j, 0, keepdims=False) for j in range(n_tp)]
    quarters = jnp.stack([mine[0]] + [swap(mine[j], "tp", j) for j in range(1, n_tp)])
    quarters = quarters.reshape(n_fs, group, w)
    base = t * lo

    def slice_for(j):
        s = (i ^ j) ^ base
        return lax.dynamic_index_in_dim(quarters, s, 0, keepdims=False)

    own = [slice_for(j) if j == 0 else swap(slice_for(j), "fs", j) for j in place]
    own = jnp.concatenate(own, axis=0)

    chunks = {0: own}
    have = [0]
    for k in reversed(range(bits_of(n_tp))):
        for g in list(have):
            chunks[g | (1 << k)] = swap(chunks[g], "tp", 1 << k)
        have = have + [g | (1 << k) for g in have]

    def by_group(a):
        a = a.reshape((n_tp, group) + a.shape[1:])
        return [lax.dynamic_index_in_dim(a, t ^ g, 0, keepdims=False) for g in range(n_tp)]

    route_groups = jnp.stack(by_group(routes)).transpose(0, 2, 1).reshape(1, n_tp, top * group)
    for k in reversed(range(n_bits)):
        route_groups = jnp.concatenate([route_groups, swap(route_groups, "fs", 1 << k)], axis=0)
    route_groups = route_groups.reshape(n_fs, n_tp, top, group).transpose(1, 0, 3, 2)
    route_groups = route_groups.reshape(n_tp, n_fs * group, top)

    token_float = tokens.astype(f32)
    full_width = w * n_fs
    sumsquares = jnp.sum(token_float * token_float, axis=1)
    for k in range(bits_of(n_tp)):
        sumsquares = sumsquares + swap(sumsquares, "tp", 1 << k)
    inverse = by_group(lax.rsqrt(sumsquares / full_width + norm_eps)[:, None])
    mix = by_group(route_weight / jnp.sum(route_weight, axis=1, keepdims=True))

    order = [0] + sorted(range(2, n_tp), key=lambda g: g) + ([1] if n_tp > 1 else [])
    half = n_fs * group // 2
    up_flops = 4 * half * w * n_experts * ff
    outs = {}
    for g in order:
        r, x = route_groups[g], chunks[g]
        shape = jax.ShapeDtypeStruct((half, 4 * ff), bf16)
        send = in_kernel(up_kernel, shape, r[half:], x[half:], gate_cast, up_cast, flops=up_flops)
        keep = in_kernel(up_kernel, shape, r[:half], x[:half], gate_cast, up_cast, flops=up_flops)
        for k in range(n_bits):
            total = keep.astype(f32) + swap(send, "fs", 1 << k).astype(f32)
            if k < n_bits - 1:
                m = total.shape[0] // 2
                total = total.astype(bf16)
                keep, send = total[:m], total[m:]
        total = total * inverse[g]
        hidden = []
        for k in range(top):
            v = total[:, 2 * k * ff : (2 * k + 1) * ff]
            u = total[:, (2 * k + 1) * ff : (2 * k + 2) * ff]
            hidden.append((jax.nn.silu(v) * u * mix[g][:, k : k + 1]).astype(bf16))
        hidden = jnp.concatenate(hidden, axis=1)
        for k in reversed(range(n_bits)):
            hidden = jnp.concatenate([hidden, swap(hidden, "fs", 1 << k)], axis=0)
        outs[g] = in_kernel(
            down_kernel,
            jax.ShapeDtypeStruct((n_fs * group, w), bf16),
            r,
            hidden,
            down_turned,
            flops=2 * n_fs * group * w * n_experts * ff,
        )

    live = n_tp
    for k in range(bits_of(n_tp)):
        bit = 1 << k
        for g in [g for g in sorted(outs) if g & bit]:
            got = swap(outs.pop(g), "tp", bit)
            outs[g ^ bit] = (outs[g ^ bit].astype(f32) + got.astype(f32)).astype(bf16)
    final = outs[0].reshape(n_fs, group, w)
    home = jnp.stack([final[p] if j == 0 else swap(final[p], "fs", j) for p, j in enumerate(place)])
    by_j = jnp.stack([home[place.index(j)] for j in range(n_fs)])
    mixed = jnp.zeros((n_tp, group, lo * w), bf16)
    for r in range(n_tp):
        parts = [
            lax.dynamic_index_in_dim(by_j, i ^ ((t ^ r) * lo + l), 0, keepdims=False)
            for l in range(lo)
        ]
        part = jnp.concatenate(parts, axis=1)
        if r:
            part = swap(part, "tp", r)
        mixed = lax.dynamic_update_index_in_dim(mixed, part, t ^ r, 0)
    mixed = mixed.reshape(rows, lo * w)

    gate_out, up_out, down_out = (
        lax.all_to_all(a, "fs", split_axis=0, concat_axis=1, tiled=True)
        for a in (gate_cast, up_cast, down_cast)
    )
    return (gate_out, up_out, down_out, mixed)


def solution(mesh):
    placed = (
        P("fs", "tp"),
        P(None, "fs", "tp"),
        P(None, "fs", "tp"),
        P(None, "fs", "tp"),
        P("fs"),
        P("fs", None),
        P("fs", None),
    )
    return jax.shard_map(
        body,
        mesh=mesh,
        in_specs=placed,
        out_specs=(P("fs", None, "tp"), P("fs", None, "tp"), P("fs", None, "tp"), P("fs", "tp")),
        check_vma=False,
    )
```

time: 342 us -> 294 us (0.86)
  blocking collectives: 129 us -> 0 us
  starting transfers between devices: 13.1 us -> 78.1 us
  Pallas kernels: 0 us -> 49.9 us
  waiting for transfers between devices: 130 us -> 94 us
  matrix products: 18.6 us -> 0 us
  other arithmetic: 16 us -> 33.6 us
  local copies, waits for them, and re-layouts: 19.7 us -> 35.7 us
  between operations: 14.3 us -> 1.29 us
    all_to_all x3 -> x0, blocking collectives: 121 us -> none  [the longest x1 75.4 us: body(): lax.all_to_all(outgoing, 'fs', split_axis=0, concat_axis=0, tiled=True)]
    ppermute x0 -> x55, waiting for transfers between devices: none -> 94 us  [swap(): return lax.ppermute(x, axis, [(s, s ^ j) for s in range(n)])]
    all_to_all x3, waiting for transfers between devices: 88.5 us -> 0.01 us  [body(): lax.all_to_all(a, 'fs', split_axis=0, concat_axis=1, tiled=True)]
    ppermute x0 -> x55, starting transfers between devices: none -> 66.7 us  [swap(): return lax.ppermute(x, axis, [(s, s ^ j) for s in range(n)])]
    pallas_call x0 -> x12, Pallas kernels: none -> 49.9 us  [in_kernel(): pl.pallas_call(body, out_shape=out, in_specs=[pl.BlockSpec(memory_space=p...]
    all_gather x2 -> x0, waiting for transfers between devices: 41.7 us -> none  [the longest x1 41.7 us: body(): segment = lax.all_gather(arrived, 'tp', axis=1, tiled=True)]
    dot_general x3 -> x0, matrix products: 18.6 us -> none  [the longest x1 7.37 us: body(): up_val = jnp.dot(segment, up_mat, preferred_element_type=jnp.float32)]
    slice x2 -> x26, local copies, waits for them, and re-layouts: 0.21 us -> 16.6 us  [the longest x5 3.9 us: body(): r[:half]]
  transfers between devices with their start and end apart: 5 -> 58, of which waited for: 3 -> 20; matrix products, arithmetic and copies ran while one was open for 6% -> 21% of each run, Pallas kernels for 0% -> 17%
where the time goes in v1:
time: 294 us; the launch traced here: 293 us
  waiting for transfers between devices  94 us (32%)
  starting transfers between devices  78.1 us (27%)
  Pallas kernels  49.9 us (17%)
  local copies, waits for them, and re-layouts  35.7 us (12%)
  other arithmetic  33.6 us (11%)
    ppermute x55, waiting for transfers between devices, swap(): return lax.ppermute(x, axis, [(s, s ^ j) for s in range(n)])  94 us
    ppermute x55, starting transfers between devices, swap(): return lax.ppermute(x, axis, [(s, s ^ j) for s in range(n)])  66.7 us
    pallas_call x12, Pallas kernels, in_kernel(): pl.pallas_call(body, out_shape=out, in_specs=[pl.BlockSpec(memory_space=p...  49.9 us
    all_to_all x3, starting transfers between devices, body(): lax.all_to_all(a, 'fs', split_axis=0, concat_axis=1, tiled=True)  11.4 us
    concatenate x12, other arithmetic, body(): hidden = jnp.concatenate([hidden, swap(hidden, 'fs', 1 << k)], axis=0)  9.03 us
    unnamed x67, local copies, waits for them, and re-layouts  8.69 us
  transfers between devices with their start and end apart: 58, of which 20 were waited for; matrix products, arithmetic and copies ran while one was open for 21% of the time, Pallas kernels for 17%

profile of v1, /device:TPU:0, one launch (start us, length us, event | category | flops | bytes accessed | tf_op | source)
XLA Modules:
  0.0 292.6 jit_solution(12045563942482747289)
XLA Ops:
  11.6 4.1 %multiply_convert_fusion = (bf16[8,512,128]{2,1,0:T(8,128)(2,1)}, bf16[8,512,128]{2,1,0:T(8,128)(2,1)}) fusion(f32[8,512,128]{2,1,0:T(8,128)} %param.9, f32[512]{0:T(512)S(1)} %copy-done.12, f32[8,512,128]{2,1,0:T(8,128)} %param.8), kind=kLoop, calls=%fused_computation | loop fusion | flops 2097152 | bytes 6293504 | tf_op jit(solution)/shard_map/convert_element_type | solution.py:108
  15.7 3.9 %all-to-all-start = ((bf16[8,512,128]{2,1,0:T(8,128)(2,1)}), bf16[8,512,128]{2,1,0:T(8,128)(2,1)S(1)}, u32[]{:S(2)}, u32[]{:S(2)}) async-start(bf16[8,512,128]{2,1,0:T(8,128)(2,1)} %get-tuple-element.73.g_ref), calls=%async_computation | async-start | bytes 2097152 | tf_op jit(solution)/shard_map/all_to_all | solution.py:205
  30.3 8.4 %collective-permute-done.1 = s32[2,4,192]{2,1,0:T(4,128)S(1)} collective-permute-done((s32[2,4,192]{2,1,0:T(4,128)S(1)}, s32[2,4,192]{2,1,0:T(4,128)S(1)}, u32[]{:S(2)}, u32[]{:S(2)}) %collective-permute-start.1) | collective-permute-done | bytes 6176 | tf_op jit(solution)/shard_map/ppermute | solution.py:19
  60.0 4.8 %collective-permute-done.10 = bf16[96,512]{1,0:T(8,128)(2,1)S(1)} collective-permute-done((bf16[96,512]{1,0:T(8,128)(2,1)S(1)}, bf16[96,512]{1,0:T(8,128)(2,1)S(1)}, u32[]{:S(2)}, u32[]{:S(2)}) %collective-permute-start.10) | collective-permute-done | bytes 98336 | tf_op jit(solution)/shard_map/ppermute | solution.py:19
  67.8 3.7 %shard_map.103 = bf16[384,512]{1,0:T(8,128)(2,1)} custom-call(s32[384,2]{1,0:T(8,128)} %bitcast.145, bf16[384,512]{1,0:T(8,128)(2,1)} %pad_maximum_fusion.2.x_ref, bf16[8,512,128]{2,1,0:T(8,128)(2,1)} %get-tuple-element.73.g_ref, bf16[8,512,128]{2,1,0:T(8,128)(2,1)} %get-tuple-element.72.u_ref), custom_call_target="tpu_custom_call" | custom-call | flops 805306368 | bytes 2493440 | tf_op jit(solution)/shard_map/pallas_call | solution.py:28
  79.2 3.7 %shard_map.102 = bf16[384,512]{1,0:T(8,128)(2,1)} custom-call(s32[384,2]{1,0:T(8,128)} %bitcast.142, bf16[384,512]{1,0:T(8,128)(2,1)} %pad_maximum_fusion.1.x_ref, bf16[8,512,128]{2,1,0:T(8,128)(2,1)} %get-tuple-element.73.g_ref, bf16[8,512,128]{2,1,0:T(8,128)(2,1)} %get-tuple-element.72.u_ref), custom_call_target="tpu_custom_call" | custom-call | flops 805306368 | bytes 2493440 | tf_op jit(solution)/shard_map/pallas_call | solution.py:28
  94.5 3.7 %shard_map.106 = bf16[384,512]{1,0:T(8,128)(2,1)} custom-call(s32[384,2]{1,0:T(8,128)} %bitcast.141, bf16[384,512]{1,0:T(8,128)(2,1)} %get-tuple-element.22.x_ref, bf16[8,512,128]{2,1,0:T(8,128)(2,1)} %get-tuple-element.73.g_ref, bf16[8,512,128]{2,1,0:T(8,128)(2,1)} %get-tuple-element.72.u_ref), custom_call_target="tpu_custom_call" | custom-call | flops 805306368 | bytes 2493440 | tf_op jit(solution)/shard_map/pallas_call | solution.py:28
  100.1 3.7 %shard_map.109 = bf16[384,512]{1,0:T(8,128)(2,1)} custom-call(s32[384,2]{1,0:T(8,128)} %bitcast.147, bf16[384,512]{1,0:T(8,128)(2,1)} %get-tuple-element.24.x_ref, bf16[8,512,128]{2,1,0:T(8,128)(2,1)} %get-tuple-element.73.g_ref, bf16[8,512,128]{2,1,0:T(8,128)(2,1)} %get-tuple-element.72.u_ref), custom_call_target="tpu_custom_call" | custom-call | flops 805306368 | bytes 2493440 | tf_op jit(solution)/shard_map/pallas_call | solution.py:28
  104.9 3.7 %shard_map.105 = bf16[384,512]{1,0:T(8,128)(2,1)} custom-call(s32[384,2]{1,0:T(8,128)} %bitcast.140, bf16[384,512]{1,0:T(8,128)(2,1)} %get-tuple-element.21.x_ref, bf16[8,512,128]{2,1,0:T(8,128)(2,1)} %get-tuple-element.73.g_ref, bf16[8,512,128]{2,1,0:T(8,128)(2,1)} %get-tuple-element.72.u_ref), custom_call_target="tpu_custom_call" | custom-call | flops 805306368 | bytes 2493440 | tf_op jit(solution)/shard_map/pallas_call | solution.py:28
  108.6 3.7 %shard_map.108 = bf16[384,512]{1,0:T(8,128)(2,1)} custom-call(s32[384,2]{1,0:T(8,128)} %bitcast.146, bf16[384,512]{1,0:T(8,128)(2,1)} %get-tuple-element.23.x_ref, bf16[8,512,128]{2,1,0:T(8,128)(2,1)} %get-tuple-element.73.g_ref, bf16[8,512,128]{2,1,0:T(8,128)(2,1)} %get-tuple-element.72.u_ref), custom_call_target="tpu_custom_call" | custom-call | flops 805306368 | bytes 2493440 | tf_op jit(solution)/shard_map/pallas_call | solution.py:28
  124.2 3.7 %shard_map.112 = bf16[384,512]{1,0:T(8,128)(2,1)} custom-call(s32[384,2]{1,0:T(8,128)} %bitcast.144, bf16[384,512]{1,0:T(8,128)(2,1)} %get-tuple-element.26.x_ref, bf16[8,512,128]{2,1,0:T(8,128)(2,1)} %get-tuple-element.73.g_ref, bf16[8,512,128]{2,1,0:T(8,128)(2,1)} %get-tuple-element.72.u_ref), custom_call_target="tpu_custom_call" | custom-call | flops 805306368 | bytes 2493440 | tf_op jit(solution)/shard_map/pallas_call | solution.py:28
  132.8 3.7 %shard_map.111 = bf16[384,512]{1,0:T(8,128)(2,1)} custom-call(s32[384,2]{1,0:T(8,128)} %bitcast.143, bf16[384,512]{1,0:T(8,128)(2,1)} %get-tuple-element.25.x_ref, bf16[8,512,128]{2,1,0:T(8,128)(2,1)} %get-tuple-element.73.g_ref, bf16[8,512,128]{2,1,0:T(8,128)(2,1)} %get-tuple-element.72.u_ref), custom_call_target="tpu_custom_call" | custom-call | flops 805306368 | bytes 2493440 | tf_op jit(solution)/shard_map/pallas_call | solution.py:28
  140.7 3.6 %all-to-all-start.1 = ((bf16[8,512,128]{2,1,0:T(8,128)(2,1)}), bf16[8,512,128]{2,1,0:T(8,128)(2,1)S(1)}, u32[]{:S(2)}, u32[]{:S(2)}) async-start(bf16[8,512,128]{2,1,0:T(8,128)(2,1)} %get-tuple-element.72.u_ref), calls=%async_computation.1 | async-start | bytes 2097152 | tf_op jit(solution)/shard_map/all_to_all | solution.py:205
  148.6 25.8 %collective-permute-done.39 = bf16[96,512]{1,0:T(8,128)(2,1)S(1)} collective-permute-done((bf16[96,512]{1,0:T(8,128)(2,1)S(1)}, bf16[96,512]{1,0:T(8,128)(2,1)S(1)}, u32[]{:S(2)}, u32[]{:S(2)}) %collective-permute-start.39) | collective-permute-done | bytes 98336 | tf_op jit(solution)/shard_map/ppermute | solution.py:19
  191.9 4.0 %all-to-all-start.2 = ((bf16[8,512,128]{1,2,0:T(8,128)(2,1)}), bf16[8,512,128]{1,2,0:T(8,128)(2,1)S(1)}, u32[]{:S(2)}, u32[]{:S(2)}) async-start(bf16[8,512,128]{1,2,0:T(8,128)(2,1)} %copy.32), calls=%async_computation.2 | async-start | bytes 2097152 | tf_op jit(solution)/shard_map/all_to_all | solution.py:205
  195.9 5.1 %shard_map.113 = bf16[768,512]{1,0:T(8,128)(2,1)} custom-call(s32[768,2]{1,0:T(8,128)} %bitcast.151, bf16[768,256]{1,0:T(8,128)(2,1)} %pad_maximum_fusion.6.h_ref, bf16[8,128,512]{2,1,0:T(8,128)(2,1)} %bitcast.32.d_ref), custom_call_target="tpu_custom_call" | custom-call | flops 805306368 | bytes 1447936 | tf_op jit(solution)/shard_map/pallas_call | solution.py:28
  204.0 9.1 %collective-permute-done.34 = bf16[192,256]{1,0:T(8,128)(2,1)S(1)} collective-permute-done((bf16[192,256]{1,0:T(8,128)(2,1)S(1)}, bf16[192,256]{1,0:T(8,128)(2,1)S(1)}, u32[]{:S(2)}, u32[]{:S(2)}) %collective-permute-start.34) | collective-permute-done | bytes 98336 | tf_op jit(solution)/shard_map/ppermute | solution.py:19
  217.6 5.1 %shard_map.107 = bf16[768,512]{1,0:T(8,128)(2,1)} custom-call(s32[768,2]{1,0:T(8,128)} %bitcast.150, bf16[768,256]{1,0:T(8,128)(2,1)} %pad_maximum_fusion.4.h_ref, bf16[8,128,512]{2,1,0:T(8,128)(2,1)} %bitcast.32.d_ref), custom_call_target="tpu_custom_call" | custom-call | flops 805306368 | bytes 1447936 | tf_op jit(solution)/shard_map/pallas_call | solution.py:28
  224.4 5.1 %shard_map.110 = bf16[768,512]{1,0:T(8,128)(2,1)} custom-call(s32[768,2]{1,0:T(8,128)} %bitcast.149, bf16[768,256]{1,0:T(8,128)(2,1)} %pad_maximum_fusion.5.h_ref, bf16[8,128,512]{2,1,0:T(8,128)(2,1)} %bitcast.32.d_ref), custom_call_target="tpu_custom_call" | custom-call | flops 805306368 | bytes 1447936 | tf_op jit(solution)/shard_map/pallas_call | solution.py:28
  232.4 4.4 %collective-permute-start.18 = (bf16[96,256]{1,0:T(8,128)(2,1)S(1)}, bf16[96,256]{1,0:T(8,128)(2,1)S(1)}, u32[]{:S(2)}, u32[]{:S(2)}) collective-permute-start(bf16[96,256]{1,0:T(8,128)(2,1)S(1)} %pad_maximum_fusion.18), channel_id=1, source_target_pairs={{0,16},{4,20},{8,24},{12,28},{16,0},{20,4},{24,8},{28,12},{1,17},{... | collective-permute-start | bytes 147464 | tf_op jit(solution)/shard_map/ppermute | solution.py:19
  240.1 4.6 %collective-permute-done.19 = bf16[192,256]{1,0:T(8,128)(2,1)S(1)} collective-permute-done((bf16[192,256]{1,0:T(8,128)(2,1)S(1)}, bf16[192,256]{1,0:T(8,128)(2,1)S(1)}, u32[]{:S(2)}, u32[]{:S(2)}) %collective-permute-start.19) | collective-permute-done | bytes 98336 | tf_op jit(solution)/shard_map/ppermute | solution.py:19
  253.3 5.1 %shard_map.104 = bf16[768,512]{1,0:T(8,128)(2,1)} custom-call(s32[768,2]{1,0:T(8,128)} %bitcast.152, bf16[768,256]{1,0:T(8,128)(2,1)} %pad_maximum_fusion.3.h_ref, bf16[8,128,512]{2,1,0:T(8,128)(2,1)} %bitcast.32.d_ref), custom_call_target="tpu_custom_call" | custom-call | flops 805306368 | bytes 1447936 | tf_op jit(solution)/shard_map/pallas_call | solution.py:28
  271.7 5.1 %collective-permute-done.48 = bf16[96,512]{1,0:T(8,128)(2,1)S(1)} collective-permute-done((bf16[96,512]{1,0:T(8,128)(2,1)S(1)}, bf16[96,512]{1,0:T(8,128)(2,1)S(1)}, u32[]{:S(2)}, u32[]{:S(2)}) %collective-permute-start.48) | collective-permute-done | bytes 98336 | tf_op jit(solution)/shard_map/ppermute | solution.py:19
  282.0 8.6 %collective-permute-done.53 = bf16[96,1024]{1,0:T(8,128)(2,1)S(1)} collective-permute-done((bf16[96,1024]{1,0:T(8,128)(2,1)S(1)}, bf16[96,1024]{1,0:T(8,128)(2,1)S(1)}, u32[]{:S(2)}, u32[]{:S(2)}) %collective-permute-start.53) | collective-permute-done | bytes 196640 | tf_op jit(solution)/shard_map/ppermute | solution.py:19
  (274 shorter events, 155.0 us)
Async XLA Ops:
  4.6 41.9 %collective-permute-start.3 = (bf16[2,96,512]{2,0,1:T(2,128)(2,1)}, bf16[2,96,512]{2,0,1:T(2,128)(2,1)}, u32[]{:S(2)}, u32[]{:S(2)}) collective-permute-start(bf16[2,96,512]{2,0,1:T(2,128)(2,1)} %get-tuple-element.37), channel_id=1, source_target_pairs={{0,1},{1,0},{2,3},{3,2},{4,5},{5,4},{6,7},{7,6},{8,9},{9,8},{10,11... | collective-permute-start | bytes 589832 | tf_op jit(solution)/shard_map/ppermute | solution.py:19
  5.1 41.4 %collective-permute-start.4 = (bf16[2,96,512]{2,0,1:T(2,128)(2,1)}, bf16[2,96,512]{2,0,1:T(2,128)(2,1)}, u32[]{:S(2)}, u32[]{:S(2)}) collective-permute-start(bf16[2,96,512]{2,0,1:T(2,128)(2,1)} %get-tuple-element.36), channel_id=1, source_target_pairs={{0,2},{1,3},{2,0},{3,1},{4,6},{5,7},{6,4},{7,5},{8,10},{9,11},{10,... | collective-permute-start | bytes 589832 | tf_op jit(solution)/shard_map/ppermute | solution.py:19
  7.6 38.9 %collective-permute-start.5 = (bf16[2,96,512]{2,0,1:T(2,128)(2,1)S(1)}, bf16[2,96,512]{2,0,1:T(2,128)(2,1)}, u32[]{:S(2)}, u32[]{:S(2)}) collective-permute-start(bf16[2,96,512]{2,0,1:T(2,128)(2,1)S(1)} %get-tuple-element.35), channel_id=1, source_target_pairs={{0,3},{1,2},{2,1},{3,0},{4,7},{5,6},{6,5},{7,4},{8,11},{9,10},{10,... | collective-permute-start | bytes 589832 | tf_op jit(solution)/shard_map/ppermute | solution.py:19
  8.0 20.2 %collective-permute-start = (s32[1,4,192]{2,1,0:T(4,128)S(1)}, s32[1,4,192]{2,1,0:T(4,128)S(1)}, u32[]{:S(2)}, u32[]{:S(2)}) collective-permute-start(s32[1,4,192]{2,1,0:T(4,128)S(1)} %reshape.81), channel_id=1, source_target_pairs={{0,16},{4,20},{8,24},{12,28},{16,0},{20,4},{24,8},{28,12},{1,17},{... | collective-permute-start | bytes 9224 | tf_op jit(solution)/shard_map/ppermute | solution.py:19
  11.6 14.3 %collective-permute-start.16 = (f32[384]{0:T(512)}, f32[384]{0:T(512)}, u32[]{:S(2)}, u32[]{:S(2)}) collective-permute-start(f32[384]{0:T(512)} %multiply_reduce_fusion), channel_id=1, source_target_pairs={{0,1},{1,0},{2,3},{3,2},{4,5},{5,4},{6,7},{7,6},{8,9},{9,8},{10,11... | collective-permute-start | bytes 4616 | tf_op jit(solution)/shard_map/ppermute | solution.py:19
  15.7 125.0 %all-to-all-start = ((bf16[8,512,128]{2,1,0:T(8,128)(2,1)}), bf16[8,512,128]{2,1,0:T(8,128)(2,1)S(1)}, u32[]{:S(2)}, u32[]{:S(2)}) async-start(bf16[8,512,128]{2,1,0:T(8,128)(2,1)} %get-tuple-element.73.g_ref), calls=%async_computation | async-start | bytes 2097152 | tf_op jit(solution)/shard_map/all_to_all | solution.py:205
  49.1 23.3 %collective-permute-start.6 = (bf16[96,512]{1,0:T(8,128)(2,1)S(1)}, bf16[96,512]{1,0:T(8,128)(2,1)S(1)}, u32[]{:S(2)}, u32[]{:S(2)}) collective-permute-start(bf16[96,512]{1,0:T(8,128)(2,1)S(1)} %get-tuple-element.33), channel_id=1, source_target_pairs={{0,16},{4,20},{8,24},{12,28},{16,0},{20,4},{24,8},{28,12},{1,17},{... | collective-permute-start | bytes 294920 | tf_op jit(solution)/shard_map/ppermute | solution.py:19
  76.9 16.6 %collective-permute-start.21 = (bf16[768,512]{1,0:T(8,128)(2,1)}, bf16[768,512]{1,0:T(8,128)(2,1)S(1)}, u32[]{:S(2)}, u32[]{:S(2)}) collective-permute-start(bf16[768,512]{1,0:T(8,128)(2,1)} %constant_dynamic-update-slice_fusion), channel_id=1, source_target_pairs={{0,1},{1,0},{2,3},{3,2},{4,5},{5,4},{6,7},{7,6},{8,9},{9,8},{10,11... | collective-permute-start | bytes 2359304 | tf_op jit(solution)/shard_map/ppermute | solution.py:19
  76.9 22.2 %collective-permute-start.29 = (bf16[768,512]{1,0:T(8,128)(2,1)}, bf16[768,512]{1,0:T(8,128)(2,1)S(1)}, u32[]{:S(2)}, u32[]{:S(2)}) collective-permute-start(bf16[768,512]{1,0:T(8,128)(2,1)} %constant_dynamic-update-slice_fusion), channel_id=1, source_target_pairs={{0,2},{1,3},{2,0},{3,1},{4,6},{5,7},{6,4},{7,5},{8,10},{9,11},{10,... | collective-permute-start | bytes 2359304 | tf_op jit(solution)/shard_map/ppermute | solution.py:19
  92.2 39.5 %collective-permute-start.15 = (bf16[96,512]{1,0:T(8,128)(2,1)}, bf16[96,512]{1,0:T(8,128)(2,1)S(1)}, u32[]{:S(2)}, u32[]{:S(2)}) collective-permute-start(bf16[96,512]{1,0:T(8,128)(2,1)} %slice.329), channel_id=1, source_target_pairs={{0,16},{4,20},{8,24},{12,28},{16,0},{20,4},{24,8},{28,12},{1,17},{... | collective-permute-start | bytes 294920 | tf_op jit(solution)/shard_map/ppermute | solution.py:19
  98.2 14.1 %collective-permute-start.22 = (bf16[384,512]{1,0:T(8,128)(2,1)}, bf16[384,512]{1,0:T(8,128)(2,1)}, u32[]{:S(2)}, u32[]{:S(2)}) collective-permute-start(bf16[384,512]{1,0:T(8,128)(2,1)} %shard_map.106), channel_id=1, source_target_pairs={{0,4},{4,0},{8,12},{12,8},{16,20},{20,16},{24,28},{28,24},{1,5},{5... | collective-permute-start | bytes 1179656 | tf_op jit(solution)/shard_map/ppermute | solution.py:19
  103.8 13.9 %collective-permute-start.30 = (bf16[384,512]{1,0:T(8,128)(2,1)}, bf16[384,512]{1,0:T(8,128)(2,1)}, u32[]{:S(2)}, u32[]{:S(2)}) collective-permute-start(bf16[384,512]{1,0:T(8,128)(2,1)} %shard_map.109), channel_id=1, source_target_pairs={{0,4},{4,0},{8,12},{12,8},{16,20},{20,16},{24,28},{28,24},{1,5},{5... | collective-permute-start | bytes 1179656 | tf_op jit(solution)/shard_map/ppermute | solution.py:19
  104.9 18.3 %collective-permute-start.36 = (bf16[768,512]{1,0:T(8,128)(2,1)S(1)}, bf16[768,512]{1,0:T(8,128)(2,1)S(1)}, u32[]{:S(2)}, u32[]{:S(2)}) collective-permute-start(bf16[768,512]{1,0:T(8,128)(2,1)S(1)} %collective-permute-done.29), channel_id=1, source_target_pairs={{0,1},{1,0},{2,3},{3,2},{4,5},{5,4},{6,7},{7,6},{8,9},{9,8},{10,11... | collective-permute-start | bytes 2359304 | tf_op jit(solution)/shard_map/ppermute | solution.py:19
  130.4 18.2 %collective-permute-start.32 = (bf16[96,512]{1,0:T(8,128)(2,1)}, bf16[96,512]{1,0:T(8,128)(2,1)}, u32[]{:S(2)}, u32[]{:S(2)}) collective-permute-start(bf16[96,512]{1,0:T(8,128)(2,1)} %slice.355), channel_id=1, source_target_pairs={{0,16},{4,20},{8,24},{12,28},{16,0},{20,4},{24,8},{28,12},{1,17},{... | collective-permute-start | bytes 294920 | tf_op jit(solution)/shard_map/ppermute | solution.py:19
  140.7 51.2 %all-to-all-start.1 = ((bf16[8,512,128]{2,1,0:T(8,128)(2,1)}), bf16[8,512,128]{2,1,0:T(8,128)(2,1)S(1)}, u32[]{:S(2)}, u32[]{:S(2)}) async-start(bf16[8,512,128]{2,1,0:T(8,128)(2,1)} %get-tuple-element.72.u_ref), calls=%async_computation.1 | async-start | bytes 2097152 | tf_op jit(solution)/shard_map/all_to_all | solution.py:205
  145.5 28.9 %collective-permute-start.39 = (bf16[96,512]{1,0:T(8,128)(2,1)S(1)}, bf16[96,512]{1,0:T(8,128)(2,1)S(1)}, u32[]{:S(2)}, u32[]{:S(2)}) collective-permute-start(bf16[96,512]{1,0:T(8,128)(2,1)S(1)} %slice.368), channel_id=1, source_target_pairs={{0,16},{4,20},{8,24},{12,28},{16,0},{20,4},{24,8},{28,12},{1,17},{... | collective-permute-start | bytes 294920 | tf_op jit(solution)/shard_map/ppermute | solution.py:19
  147.3 28.3 %collective-permute-start.25 = (bf16[96,256]{1,0:T(8,128)(2,1)S(1)}, bf16[96,256]{1,0:T(8,128)(2,1)S(1)}, u32[]{:S(2)}, u32[]{:S(2)}) collective-permute-start(bf16[96,256]{1,0:T(8,128)(2,1)S(1)} %pad_maximum_fusion.19), channel_id=1, source_target_pairs={{0,16},{4,20},{8,24},{12,28},{16,0},{20,4},{24,8},{28,12},{1,17},{... | collective-permute-start | bytes 147464 | tf_op jit(solution)/shard_map/ppermute | solution.py:19
  182.5 33.3 %collective-permute-start.27 = (bf16[384,256]{1,0:T(8,128)(2,1)}, bf16[384,256]{1,0:T(8,128)(2,1)}, u32[]{:S(2)}, u32[]{:S(2)}) collective-permute-start(bf16[384,256]{1,0:T(8,128)(2,1)} %pad_maximum_fusion.8), channel_id=1, source_target_pairs={{0,4},{4,0},{8,12},{12,8},{16,20},{20,16},{24,28},{28,24},{1,5},{5... | collective-permute-start | bytes 589832 | tf_op jit(solution)/shard_map/ppermute | solution.py:19
  187.6 13.3 %collective-permute-start.33 = (bf16[96,256]{1,0:T(8,128)(2,1)}, bf16[96,256]{1,0:T(8,128)(2,1)}, u32[]{:S(2)}, u32[]{:S(2)}) collective-permute-start(bf16[96,256]{1,0:T(8,128)(2,1)} %pad_maximum_fusion.20), channel_id=1, source_target_pairs={{0,16},{4,20},{8,24},{12,28},{16,0},{20,4},{24,8},{28,12},{1,17},{... | collective-permute-start | bytes 147464 | tf_op jit(solution)/shard_map/ppermute | solution.py:19
  191.9 55.1 %all-to-all-start.2 = ((bf16[8,512,128]{1,2,0:T(8,128)(2,1)}), bf16[8,512,128]{1,2,0:T(8,128)(2,1)S(1)}, u32[]{:S(2)}, u32[]{:S(2)}) async-start(bf16[8,512,128]{1,2,0:T(8,128)(2,1)} %copy.32), calls=%async_computation.2 | async-start | bytes 2097152 | tf_op jit(solution)/shard_map/all_to_all | solution.py:205
  201.0 28.5 %collective-permute-start.43 = (bf16[768,512]{1,0:T(8,128)(2,1)}, bf16[768,512]{1,0:T(8,128)(2,1)}, u32[]{:S(2)}, u32[]{:S(2)}) collective-permute-start(bf16[768,512]{1,0:T(8,128)(2,1)} %shard_map.113), channel_id=1, source_target_pairs={{0,1},{1,0},{2,3},{3,2},{4,5},{5,4},{6,7},{7,6},{8,9},{9,8},{10,11... | collective-permute-start | bytes 2359304 | tf_op jit(solution)/shard_map/ppermute | solution.py:19
  222.7 35.6 %collective-permute-start.28 = (bf16[768,512]{1,0:T(8,128)(2,1)}, bf16[768,512]{1,0:T(8,128)(2,1)}, u32[]{:S(2)}, u32[]{:S(2)}) collective-permute-start(bf16[768,512]{1,0:T(8,128)(2,1)} %shard_map.107), channel_id=1, source_target_pairs={{0,1},{1,0},{2,3},{3,2},{4,5},{5,4},{6,7},{7,6},{8,9},{9,8},{10,11... | collective-permute-start | bytes 2359304 | tf_op jit(solution)/shard_map/ppermute | solution.py:19
  231.9 26.4 %collective-permute-start.44 = (bf16[768,512]{1,0:T(8,128)(2,1)}, bf16[768,512]{1,0:T(8,128)(2,1)}, u32[]{:S(2)}, u32[]{:S(2)}) collective-permute-start(bf16[768,512]{1,0:T(8,128)(2,1)} %add_convert_fusion.1), channel_id=1, source_target_pairs={{0,2},{1,3},{2,0},{3,1},{4,6},{5,7},{6,4},{7,5},{8,10},{9,11},{10,... | collective-permute-start | bytes 2359304 | tf_op jit(solution)/shard_map/ppermute | solution.py:19
  265.6 13.3 %collective-permute-start.49 = (bf16[96,512]{1,0:T(8,128)(2,1)S(1)}, bf16[96,512]{1,0:T(8,128)(2,1)S(1)}, u32[]{:S(2)}, u32[]{:S(2)}) collective-permute-start(bf16[96,512]{1,0:T(8,128)(2,1)S(1)} %get-tuple-element.16), channel_id=1, source_target_pairs={{0,20},{4,16},{8,28},{12,24},{16,4},{20,0},{24,12},{28,8},{1,21},{... | collective-permute-start | bytes 294920 | tf_op jit(solution)/shard_map/ppermute | solution.py:19
  (59 other events, 629.5 us)
